TPU v7x, 32 devices: a whole 2x2x4 slice. The times are simulated.
32 devices in a mesh: rep: 2 (over x), fs: 8 (over z, y), tp: 2 (over core).
Axes of the slice: x: 2, y: 2, z: 4, core: 2. Of those that a mesh axis runs over, the one named last changes fastest.
Arguments:
- inputs: bfloat16 [8192, 2048], P(('rep', 'fs')), may hold values from -6 to 6
- gain: float32 [2048], replicated, may hold values from 0.1 to 1.9
- gate_weight: bfloat16 [2048, 3072], P('fs', 'tp'), may hold values from -0.125 to 0.125
- up_weight: bfloat16 [2048, 3072], P('fs', 'tp'), may hold values from -0.125 to 0.125
- down_weight: bfloat16 [2048, 3072], P('fs', 'tp'), may hold values from -0.109375 to 0.109375
- cotangent: bfloat16 [8192, 2048], P(('rep', 'fs')), may hold values from -6 to 6
Outputs:
- input_gradient: bfloat16 [8192, 2048], P(('rep', 'fs'))
- gain_gradient: float32 [2048], replicated
- d_down: float32 [2048, 3072], P('fs', 'tp')
All inputs are finite; a program needn't handle non-finite values.
Results may differ from a plain program's by a relative error of at most 0.014.
Values may be sent and summed in bfloat16 or wider, within the bound.
A program may use at most 128 MiB of HBM per device.

v0:
```python
import jax
import jax.numpy as jnp
from jax import lax
from jax.sharding import PartitionSpec as P

EPS = 1e-06


def local(inputs, gain, gate_weight, up_weight, down_weight, cotangent):
    single_precision = inputs.astype(jnp.float32)
    reciprocal_root_mean = lax.rsqrt(
        jnp.mean(single_precision * single_precision, axis=-1, keepdims=True) + EPS
    )
    unit_input = single_precision * reciprocal_root_mean
    normalized_input = (unit_input * gain).astype(jnp.bfloat16)
    row_count = inputs.shape[0]
    contract_cols = (((1,), (1,)), ((), ()))
    gate_full, up_full, down_full = (
        lax.all_gather(gate_weight, "fs", axis=0, tiled=True),
        lax.all_gather(up_weight, "fs", axis=0, tiled=True),
        lax.all_gather(down_weight, "fs", axis=0, tiled=True),
    )
    gate = jnp.dot(normalized_input, gate_full, preferred_element_type=jnp.float32)
    up_proj = jnp.dot(normalized_input, up_full, preferred_element_type=jnp.float32)
    down_sum = jnp.dot(cotangent, down_full, preferred_element_type=jnp.float32)
    gate_sig = jax.nn.sigmoid(gate)
    active = gate * gate_sig
    hidden = (active * up_proj).astype(jnp.bfloat16)
    d_hidden = 0.5 * down_sum
    d_gate = (d_hidden * up_proj * gate_sig * (1.0 + gate * (1.0 - gate_sig))).astype(jnp.bfloat16)
    d_up = (d_hidden * active).astype(jnp.bfloat16)
    partial_value = lax.dot_general(
        d_gate, gate_full, contract_cols, preferred_element_type=jnp.float32
    ) + lax.dot_general(d_up, up_full, contract_cols, preferred_element_type=jnp.float32)
    summed_units = lax.psum(partial_value.astype(jnp.bfloat16), "tp")
    normalized_gradient = summed_units.astype(jnp.float32)
    gain_gradient = lax.psum(jnp.sum(normalized_gradient * unit_input, axis=0), ("rep", "fs"))
    gain_scaled = gain * normalized_gradient
    mean_correction = jnp.mean(gain_scaled * unit_input, axis=-1, keepdims=True)
    input_gradient = (
        cotangent.astype(jnp.float32)
        + reciprocal_root_mean * (gain_scaled - unit_input * mean_correction)
    ).astype(jnp.bfloat16)
    contract_rows = (((0,), (0,)), ((), ()))
    width = cotangent.shape[1]
    groups_fs = lax.axis_size("fs")
    groups_rep = lax.axis_size("rep")
    sub_rows = width // (groups_fs * groups_rep)
    reordered = (
        cotangent.reshape(row_count, groups_fs, groups_rep, sub_rows)
        .transpose(0, 2, 1, 3)
        .reshape(row_count, width)
    )
    summed = lax.psum_scatter(
        0.5 * lax.dot_general(reordered, hidden, contract_rows, preferred_element_type=jnp.float32),
        ("rep", "fs"),
        scatter_dimension=0,
        tiled=True,
    )
    d_down = lax.all_gather(summed, "rep", axis=0, tiled=True)
    return (input_gradient, gain_gradient, d_down)


def solution(mesh):
    placed = (
        P(("rep", "fs"), None),
        P(),
        P("fs", "tp"),
        P("fs", "tp"),
        P("fs", "tp"),
        P(("rep", "fs"), None),
    )
    return jax.shard_map(
        local,
        mesh=mesh,
        in_specs=placed,
        out_specs=(P(("rep", "fs"), None), P(), P("fs", "tp")),
        check_vma=False,
    )
```

profile of v0, /device:TPU:0, one launch (start us, length us, event | category | flops | bytes accessed | tf_op | source)
XLA Modules:
  0.0 600.7 jit_solution(4841965839708579481)
XLA Ops:
  7.2 0.0 copy-start.1
  7.2 0.0 all-gather.9.cloned.1.call-start
  7.2 0.7 all-gather.9.cloned.1.call-update
  7.9 0.0 all-gather.7.cloned.1.call-start
  8.0 0.7 all-gather.7.cloned.1.call-update
  8.7 0.0 all-gather.5.cloned.1.call-start
  8.7 0.7 all-gather.5.cloned.1.call-update
  9.4 0.0 reduce-scatter.2.cloned.1.call-start
  9.4 0.0 copy-done.1
  9.5 2.5 copy.11
  12.0 0.0 copy-start
  12.0 0.0 copy-start.3
  12.0 3.3 copy.12
  15.2 0.0 copy-done
  15.2 0.5 fusion.9
  15.7 95.9 %all-gather.9.cloned.1.call-done = bf16[2048,1536]{1,0:T(8,128)(2,1)} async-done(((bf16[256,1536]{1,0:T(8,128)(2,1)}), bf16[2048,1536]{1,0:T(8,128)(2,1)}) %all-gather.9.cloned.1.call-update) | async-done | bytes 6291472 | tf_op jit(solution)/shard_map/all_gather | solution.py:19
  111.6 0.0 copy-done.3
  111.6 7.9 %fusion.14 = f32[512,1536]{1,0:T(8,128)} fusion(bf16[2048,1536]{1,0:T(8,128)(2,1)} %all-gather.9.cloned.1.call-done, bf16[512,2048]{1,0:T(8,128)(2,1)S(1)} %copy-done, f32[2048]{0:T(1024)S(1)} %copy-done.3, f32[512]{0:T(512)S(1)} %add_rsqrt_fusion), kind=kOutput, calls=%fused_computation.25 | convolution fusion | flops 3225419776 | bytes 11544576 | tf_op jit(solution)/shard_map/dot_general | solution.py:23
  119.5 91.2 %all-gather.7.cloned.1.call-done = bf16[2048,1536]{1,0:T(8,128)(2,1)} async-done(((bf16[256,1536]{1,0:T(8,128)(2,1)}), bf16[2048,1536]{1,0:T(8,128)(2,1)}) %all-gather.7.cloned.1.call-update) | async-done | bytes 6291472 | tf_op jit(solution)/shard_map/all_gather | solution.py:20
  210.7 0.0 copy-start.2
  210.7 0.0 copy-start.4
  210.7 5.8 fusion.16
  216.5 0.0 copy-start.6
  216.5 1.7 copy-done.6
  218.2 0.0 copy-done.2
  218.2 0.0 copy-done.4
  218.2 6.8 %multiply_bitcast_fusion = f32[2048,1536]{0,1:T(8,128)} fusion(bf16[512,2048]{0,1:T(8,128)(2,1)S(1)} %bitcast.14, f32[512,1536]{1,0:T(8,128)S(1)} %fusion.16, f32[512,1536]{1,0:T(8,128)S(1)} %copy-done.4), kind=kOutput, calls=%fused_computation | convolution fusion | flops 3229089792 | bytes 20971520 | tf_op jit(solution)/shard_map/dot_general | solution.py:55
  225.1 0.0 reduce-scatter.2.cloned.1.call-update
  225.1 0.2 all-reduce.2.cloned.1.call-start
  225.3 84.5 %all-gather.5.cloned.1.call-done = bf16[2048,1536]{1,0:T(8,128)(2,1)} async-done(((bf16[256,1536]{1,0:T(8,128)(2,1)}), bf16[2048,1536]{1,0:T(8,128)(2,1)}) %all-gather.5.cloned.1.call-update) | async-done | bytes 6291472 | tf_op jit(solution)/shard_map/all_gather | solution.py:21
  309.8 0.0 copy-start.5
  309.8 0.0 slice-start
  309.8 8.6 %convolution_multiply_fusion = f32[512,1536]{1,0:T(8,128)} fusion(bf16[512,2048]{1,0:T(8,128)(2,1)} %param.11, bf16[2048,1536]{1,0:T(8,128)(2,1)} %all-gather.5.cloned.1.call-done), kind=kOutput, calls=%fused_computation.17 | convolution fusion | flops 3222011904 | bytes 11534336 | tf_op jit(solution)/shard_map/dot_general | solution.py:25
  318.4 0.0 copy-done.5
  318.4 0.0 copy-done.7
  318.4 8.6 %fusion.12 = f32[512,2048]{1,0:T(8,128)S(1)} fusion(bf16[2048,1536]{1,0:T(8,128)(2,1)} %all-gather.9.cloned.1.call-done, f32[512,1536]{1,0:T(8,128)S(1)} %copy-done.5, f32[512,1536]{1,0:T(8,128)} %convolution_multiply_fusion, f32[512,1536]{1,0:T(8,128)S(1)} %copy-done.7), kind=kOutput, calls=%fused_computation.23 | convolution fusion | flops 3229089792 | bytes 19922944 | tf_op jit(solution)/shard_map/dot_general | solution.py:32
  327.0 0.0 slice-done
  327.0 0.0 slice-done.1
  327.1 6.6 %add_convert_fusion = bf16[512,2048]{1,0:T(8,128)(2,1)} fusion(f32[512,2048]{1,0:T(8,128)S(1)} %fusion.12, bf16[2048,1536]{1,0:T(8,128)(2,1)S(1)} %bitcast.16, f32[512,1536]{1,0:T(8,128)} %convolution_multiply_fusion, f32[512,1536]{1,0:T(8,128)S(1)} %copy-done.5), kind=kOutput, calls=%fused_computation.16 | convolution fusion | flops 3228041216 | bytes 18874368 | tf_op jit(solution)/shard_map/dot_general | solution.py:34
  333.7 0.0 all-reduce.2.cloned.1.call-update
  333.7 0.0 all-gather.11.cloned.1.call-start
  333.7 182.3 %reduce-scatter.2.cloned.1.call-done = f32[128,1536]{0,1:T(8,128)} async-done(((f32[2048,1536]{0,1:T(8,128)}), f32[128,1536]{0,1:T(8,128)}) %reduce-scatter.2.cloned.1.call-update) | async-done | bytes 786448 | tf_op jit(solution)/shard_map/reduce_scatter | solution.py:54
  516.0 0.0 all-gather.11.cloned.1.call-update
  516.1 23.6 %all-reduce.2.cloned.1.call-done = bf16[512,2048]{1,0:T(8,128)(2,1)} async-done(((bf16[512,2048]{1,0:T(8,128)(2,1)}), bf16[512,2048]{1,0:T(8,128)(2,1)}) %all-reduce.2.cloned.1.call-update) | async-done | bytes 2097168 | tf_op jit(solution)/shard_map/psum | solution.py:35
  539.6 2.9 fusion.10
  542.5 43.3 %psum.15 = f32[2048]{0:T(1024)} all-reduce(f32[2048]{0:T(1024)S(1)} %get-tuple-element.12), channel_id=1, replica_groups=mesh['rep'=2,'fs'=8,'tp'=2] {'rep','fs'}, use_global_device_ids=true, to_apply=%region_4.0 | all-reduce | flops 2048 | bytes 16384 | tf_op jit(solution)/shard_map/psum | solution.py:37
  585.8 5.0 fusion.6
  590.8 3.0 copy.13
  (6 shorter events, 0.0 us)
Async XLA Ops:
  7.2 2.3 copy-start.1
  7.2 104.4 %all-gather.9.cloned.1.call-start = ((), (), s32[]{:S(2)}) async-start(), calls=%async_computation.3 | async-start | bytes 7077888 | tf_op jit(solution)/shard_map/all_gather | solution.py:19
  7.9 202.8 %all-gather.7.cloned.1.call-start = ((), (), s32[]{:S(2)}) async-start(), calls=%async_computation.2 | async-start | bytes 7077888 | tf_op jit(solution)/shard_map/all_gather | solution.py:20
  8.7 301.1 %all-gather.5.cloned.1.call-start = ((), (), s32[]{:S(2)}) async-start(), calls=%async_computation.1 | async-start | bytes 7077888 | tf_op jit(solution)/shard_map/all_gather | solution.py:21
  9.4 506.6 %reduce-scatter.2.cloned.1.call-start = ((), (), s32[]{:S(2)}) async-start(), calls=%async_computation.5 | async-start | bytes 13369344 | tf_op jit(solution)/shard_map/reduce_scatter | solution.py:54
  12.0 3.3 copy-start
  12.0 99.7 %copy-start.3 = (f32[2048]{0:T(1024)S(1)}, f32[2048]{0:T(1024)}, u32[]{:S(2)}) copy-start(f32[2048]{0:T(1024)} %param.7) | copy-start | bytes 24580
  210.7 7.5 %copy-start.2 = (bf16[512,2,8,128]{0,3,2,1:T(8,128)(2,1)S(1)}, bf16[512,2,8,128]{0,3,2,1:T(8,128)(2,1)}, u32[]{:S(2)}) copy-start(bf16[512,2,8,128]{0,3,2,1:T(8,128)(2,1)} %copy.12) | copy-start | bytes 6291460
  210.7 7.5 %copy-start.4 = (f32[512,1536]{1,0:T(8,128)S(1)}, f32[512,1536]{1,0:T(8,128)}, u32[]{:S(2)}) copy-start(f32[512,1536]{1,0:T(8,128)} %fusion.14) | copy-start | bytes 9437188
  216.5 1.8 copy-start.6
  225.1 314.5 %all-reduce.2.cloned.1.call-start = ((), (), s32[]{:S(2)}) async-start(), calls=%async_computation.4 | async-start | bytes 4194304 | tf_op jit(solution)/shard_map/psum | solution.py:35
  309.8 8.6 %copy-start.5 = (f32[512,1536]{1,0:T(8,128)S(1)}, f32[512,1536]{1,0:T(8,128)}, u32[]{:S(2)}) copy-start(f32[512,1536]{1,0:T(8,128)} %fusion.14) | copy-start | bytes 9437188
  309.8 8.6 %copy-start.7 = (f32[512,1536]{1,0:T(8,128)S(1)}, f32[512,1536]{1,0:T(8,128)}, u32[]{:S(2)}) copy-start(f32[512,1536]{1,0:T(8,128)} %copy-done.6) | copy-start | bytes 9437188
  309.8 17.2 %slice-start = ((s8[6291456]{0:T(1024)(128)(4,1)}), s8[4194304]{0:T(1024)(128)(4,1)S(1)}, s32[]{:S(2)}) async-start(s8[6291456]{0:T(1024)(128)(4,1)} %bitcast.15), calls=%async_computation.7 | async-start | bytes 8388608
  318.4 8.6 %slice-start.1 = ((s8[6291456]{0:T(1024)(128)(4,1)}), s8[2097152]{0:T(1024)(128)(4,1)S(1)}, s32[]{:S(2)}) async-start(s8[6291456]{0:T(1024)(128)(4,1)} %bitcast.15), calls=%async_computation.8 | async-start | bytes 4194304
  333.7 257.1 %all-gather.11.cloned.1.call-start = ((), (), s32[]{:S(2)}) async-start(), calls=%async_computation.6 | async-start | bytes 2359296 | tf_op jit(solution)/shard_map/all_gather | solution.py:60
Sparse Core Ops, SparseCore 0:
  10.2 101.4 all-gather.8
  113.8 96.8 all-gather.6
  212.9 96.8 all-gather.4
  315.3 200.6 reduce-scatter.1
  518.8 20.7 all-reduce.1
  541.0 28.3 all-gather.10
where the time goes:
time: 601 us
  waiting for transfers between devices  480 us (80%)
  matrix products  44.2 us (7%)
  blocking collectives  43.3 us (7%)
  between operations  14.2 us (2%)
  local copies, waits for them, and re-layouts  10.6 us (2%)
  other arithmetic  8.39 us (1%)
    reduce_scatter x1, waiting for transfers between devices, local(): lax.psum_scatter(0.5 * lax.dot_general(reordered, hidden, contract_rows,...  182 us
    all_gather x1, waiting for transfers between devices, local(): lax.all_gather(gate_weight, 'fs', axis=0, tiled=True)  95.9 us
    all_gather x1, waiting for transfers between devices, local(): lax.all_gather(up_weight, 'fs', axis=0, tiled=True)  91.2 us
    all_gather x1, waiting for transfers between devices, local(): lax.all_gather(down_weight, 'fs', axis=0, tiled=True)  84.5 us
    psum x1, blocking collectives, local(): lax.psum(jnp.sum(normalized_gradient * unit_input, axis=0), ('rep', 'fs'))  43.3 us
    psum x1, waiting for transfers between devices, local(): summed_units = lax.psum(partial_value.astype(jnp.bfloat16), 'tp')  23.6 us
  transfers between devices with their start and end apart: 6, of which 5 were waited for; matrix products, arithmetic and copies ran while one was open for 10% of the time, Pallas kernels for 0%

commit v1 on v0

--- a/solution.py
+++ b/solution.py
@@ -4,6 +4,27 @@
 from jax.sharding import PartitionSpec as P
 
 EPS = 1e-06
+
+
+def gather_around(x, axis, dim):
+    size, mine, rows = (lax.axis_size(axis), lax.axis_index(axis), x.shape[dim])
+    ahead = [(i, (i + 1) % size) for i in range(size)]
+    left = [(i, (i - 1) % size) for i in range(size)]
+    filled = jnp.zeros((*x.shape[:dim], size * rows, *x.shape[dim + 1 :]), x.dtype)
+    filled = lax.dynamic_update_slice_in_dim(filled, x, mine * rows, axis=dim)
+    from_left = from_right = x
+    half = size // 2
+    for step in range(1, half + 1):
+        from_left = lax.ppermute(from_left, axis, ahead)
+        filled = lax.dynamic_update_slice_in_dim(
+            filled, from_left, (mine - step) % size * rows, axis=dim
+        )
+        if step < size - half:
+            from_right = lax.ppermute(from_right, axis, left)
+            filled = lax.dynamic_update_slice_in_dim(
+                filled, from_right, (mine + step) % size * rows, axis=dim
+            )
+    return filled
 
 
 def local(inputs, gain, gate_weight, up_weight, down_weight, cotangent):
@@ -17,7 +38,7 @@
     contract_cols = (((1,), (1,)), ((), ()))
     gate_full, up_full, down_full = (
         lax.all_gather(gate_weight, "fs", axis=0, tiled=True),
-        lax.all_gather(up_weight, "fs", axis=0, tiled=True),
+        gather_around(up_weight, "fs", 0),
         lax.all_gather(down_weight, "fs", axis=0, tiled=True),
     )
     gate = jnp.dot(normalized_input, gate_full, preferred_element_type=jnp.float32)

time: 601 us -> 581 us (0.967)
  waiting for transfers between devices: 480 us -> 432 us
  starting transfers between devices: 0.42 us -> 21.9 us
  local copies, waits for them, and re-layouts: 10.6 us -> 18.3 us
    ppermute x0 -> x7, waiting for transfers between devices: none -> 147 us  [the longest x4 141 us: gather_around(): from_left = lax.ppermute(from_left, axis, ahead)]
    all_gather x1, waiting for transfers between devices: 95.9 us -> 0.01 us  [local(): lax.all_gather(gate_weight, 'fs', axis=0, tiled=True)]
    all_gather x1 -> x0, waiting for transfers between devices: 91.2 us -> none  [local(): lax.all_gather(up_weight, 'fs', axis=0, tiled=True)]
    ppermute x0 -> x7, starting transfers between devices: none -> 21.5 us  [the longest x3 11 us: gather_around(): from_right = lax.ppermute(from_right, axis, left)]
    all_gather x1, waiting for transfers between devices: 84.5 us -> 76.6 us  [local(): lax.all_gather(down_weight, 'fs', axis=0, tiled=True)]
  transfers between devices with their start and end apart: 6 -> 12, of which waited for: 5 -> 8; matrix products, arithmetic and copies ran while one was open for 10% -> 11% of each run, Pallas kernels for 0% -> 0%
where the time goes in v1:
time: 581 us
  waiting for transfers between devices  432 us (74%)
  blocking collectives  43.3 us (7%)
  matrix products  41.7 us (7%)
  starting transfers between devices  21.9 us (4%)
  local copies, waits for them, and re-layouts  18.3 us (3%)
  between operations  13.9 us (2%)
  other arithmetic  9.98 us (2%)
    reduce_scatter x1, waiting for transfers between devices, local(): lax.psum_scatter(0.5 * lax.dot_general(reordered, hidden, contract_rows,...  183 us
    ppermute x4, waiting for transfers between devices, gather_around(): from_left = lax.ppermute(from_left, axis, ahead)  141 us
    all_gather x1, waiting for transfers between devices, local(): lax.all_gather(down_weight, 'fs', axis=0, tiled=True)  76.6 us
    psum x1, blocking collectives, local(): lax.psum(jnp.sum(normalized_gradient * unit_input, axis=0), ('rep', 'fs'))  43.3 us
    psum x1, waiting for transfers between devices, local(): summed_units = lax.psum(partial_value.astype(jnp.bfloat16), 'tp')  23.6 us
  transfers between devices with their start and end apart: 12, of which 8 were waited for; matrix products, arithmetic and copies ran while one was open for 11% of the time, Pallas kernels for 0%

profile of v1, /device:TPU:0, one launch (start us, length us, event | category | flops | bytes accessed | tf_op | source)
XLA Modules:
  0.0 580.6 jit_solution(8786182151702985928)
XLA Ops:
  7.2 0.0 all-gather.6.cloned.1.call-start
  7.2 0.7 all-gather.6.cloned.1.call-update
  7.9 0.0 all-gather.4.cloned.1.call-start
  8.0 0.7 all-gather.4.cloned.1.call-update
  8.7 0.0 reduce-scatter.2.cloned.1.call-start
  8.7 3.0 collective-permute-start
  11.8 3.1 collective-permute-start.1
  14.9 39.3 %collective-permute-done = bf16[256,1536]{1,0:T(8,128)(2,1)S(1)} collective-permute-done((bf16[256,1536]{1,0:T(8,128)(2,1)}, bf16[256,1536]{1,0:T(8,128)(2,1)S(1)}, u32[]{:S(2)}, u32[]{:S(2)}) %collective-permute-start) | collective-permute-done | bytes 786464 | tf_op jit(solution)/shard_map/ppermute | solution.py:18
  54.2 2.4 collective-permute-start.2
  56.5 3.9 collective-permute-start.3
  60.4 2.1 fusion.9
  62.5 42.3 %collective-permute-done.2 = bf16[256,1536]{1,0:T(8,128)(2,1)} collective-permute-done((bf16[256,1536]{1,0:T(8,128)(2,1)S(1)}, bf16[256,1536]{1,0:T(8,128)(2,1)}, u32[]{:S(2)}, u32[]{:S(2)}) %collective-permute-start.2) | collective-permute-done | bytes 786464 | tf_op jit(solution)/shard_map/ppermute | solution.py:18
  104.8 2.6 collective-permute-start.4
  107.4 2.5 copy.11
  109.9 3.1 copy.12
  113.0 0.4 broadcast_in_dim.2
  113.4 0.7 copy-done.4
  114.2 0.1 constant_dynamic-update-slice_fusion.7
  114.2 0.2 copy-done.6
  114.4 0.1 constant_dynamic-update-slice_fusion.6
  114.5 4.0 collective-permute-start.5
  118.5 1.2 constant_dynamic-update-slice_fusion.5
  119.7 38.4 %collective-permute-done.4 = bf16[256,1536]{1,0:T(8,128)(2,1)} collective-permute-done((bf16[256,1536]{1,0:T(8,128)(2,1)}, bf16[256,1536]{1,0:T(8,128)(2,1)}, u32[]{:S(2)}, u32[]{:S(2)}) %collective-permute-start.4) | collective-permute-done | bytes 786464 | tf_op jit(solution)/shard_map/ppermute | solution.py:18
  158.1 2.5 collective-permute-start.6
  160.6 1.2 constant_dynamic-update-slice_fusion.4
  161.8 0.1 constant_dynamic-update-slice_fusion.3
  161.9 1.3 constant_dynamic-update-slice_fusion.2
  163.2 5.8 collective-permute-done.5
  169.0 0.1 constant_dynamic-update-slice_fusion.1
  169.0 21.4 %collective-permute-done.6 = bf16[256,1536]{1,0:T(8,128)(2,1)S(1)} collective-permute-done((bf16[256,1536]{1,0:T(8,128)(2,1)}, bf16[256,1536]{1,0:T(8,128)(2,1)S(1)}, u32[]{:S(2)}, u32[]{:S(2)}) %collective-permute-start.6) | collective-permute-done | bytes 786464 | tf_op jit(solution)/shard_map/ppermute | solution.py:18
  190.4 0.1 constant_dynamic-update-slice_fusion
  190.5 2.7 copy-done.2
  193.2 5.2 fusion.16
  198.4 6.0 %fusion.14 = f32[512,1536]{1,0:T(8,128)S(1)} fusion(bf16[2048,1536]{1,0:T(8,128)(2,1)} %all-gather.6.cloned.1.call-done, bf16[512,2048]{1,0:T(8,128)(2,1)S(1)} %copy-done, f32[2048]{0:T(1024)S(1)} %copy-done.7, f32[512]{0:T(512)S(1)} %add_rsqrt_fusion), kind=kOutput, calls=%fused_computation.25 | convolution fusion | flops 3225419776 | bytes 11544576 | tf_op jit(solution)/shard_map/dot_general | solution.py:44
  204.3 1.6 copy-done.10
  206.0 6.8 %multiply_bitcast_fusion = f32[2048,1536]{0,1:T(8,128)} fusion(bf16[512,2048]{0,1:T(8,128)(2,1)S(1)} %bitcast.16, f32[512,1536]{1,0:T(8,128)S(1)} %copy-done.8, f32[512,1536]{1,0:T(8,128)S(1)} %fusion.14), kind=kOutput, calls=%fused_computation | convolution fusion | flops 3229089792 | bytes 20971520 | tf_op jit(solution)/shard_map/dot_general | solution.py:76
  212.8 0.2 all-reduce.2.cloned.1.call-start
  213.1 76.6 %all-gather.4.cloned.1.call-done = bf16[2048,1536]{1,0:T(8,128)(2,1)} async-done(((bf16[256,1536]{1,0:T(8,128)(2,1)}), bf16[2048,1536]{1,0:T(8,128)(2,1)}) %all-gather.4.cloned.1.call-update) | async-done | bytes 6291472 | tf_op jit(solution)/shard_map/all_gather | solution.py:42
  289.7 8.6 %convolution_multiply_fusion = f32[512,1536]{1,0:T(8,128)} fusion(bf16[512,2048]{1,0:T(8,128)(2,1)} %param.11, bf16[2048,1536]{1,0:T(8,128)(2,1)} %all-gather.4.cloned.1.call-done), kind=kOutput, calls=%fused_computation.17 | convolution fusion | flops 3222011904 | bytes 11534336 | tf_op jit(solution)/shard_map/dot_general | solution.py:46
  298.3 8.5 %fusion.12 = f32[512,2048]{1,0:T(8,128)S(1)} fusion(bf16[2048,1536]{1,0:T(8,128)(2,1)} %all-gather.6.cloned.1.call-done, f32[512,1536]{1,0:T(8,128)S(1)} %copy-done.11, f32[512,1536]{1,0:T(8,128)} %convolution_multiply_fusion, f32[512,1536]{1,0:T(8,128)S(1)} %copy-done.9), kind=kOutput, calls=%fused_computation.23 | convolution fusion | flops 3229089792 | bytes 19922944 | tf_op jit(solution)/shard_map/dot_general | solution.py:53
  306.8 6.6 %add_convert_fusion = bf16[512,2048]{1,0:T(8,128)(2,1)} fusion(f32[512,2048]{1,0:T(8,128)S(1)} %fusion.12, bf16[2048,1536]{1,0:T(8,128)(2,1)S(1)} %bitcast.15, f32[512,1536]{1,0:T(8,128)} %convolution_multiply_fusion, f32[512,1536]{1,0:T(8,128)S(1)} %copy-done.11), kind=kOutput, calls=%fused_computation.16 | convolution fusion | flops 3228041216 | bytes 18874368 | tf_op jit(solution)/shard_map/dot_general | solution.py:55
  313.5 0.0 all-gather.8.cloned.1.call-start
  313.5 182.8 %reduce-scatter.2.cloned.1.call-done = f32[128,1536]{0,1:T(8,128)} async-done(((f32[2048,1536]{0,1:T(8,128)}), f32[128,1536]{0,1:T(8,128)}) %reduce-scatter.2.cloned.1.call-update) | async-done | bytes 786448 | tf_op jit(solution)/shard_map/reduce_scatter | solution.py:75
  496.3 23.6 %all-reduce.2.cloned.1.call-done = bf16[512,2048]{1,0:T(8,128)(2,1)} async-done(((bf16[512,2048]{1,0:T(8,128)(2,1)}), bf16[512,2048]{1,0:T(8,128)(2,1)}) %all-reduce.2.cloned.1.call-update) | async-done | bytes 2097168 | tf_op jit(solution)/shard_map/psum | solution.py:56
  519.9 2.9 fusion.10
  522.8 43.3 %psum.15 = f32[2048]{0:T(1024)} all-reduce(f32[2048]{0:T(1024)S(1)} %get-tuple-element.12), channel_id=1, replica_groups=mesh['rep'=2,'fs'=8,'tp'=2] {'rep','fs'}, use_global_device_ids=true, to_apply=%region_4.5 | all-reduce | flops 2048 | bytes 16384 | tf_op jit(solution)/shard_map/psum | solution.py:58
  566.1 5.0 fusion.6
  571.1 3.0 copy.13
  (34 shorter events, 0.1 us)
Async XLA Ops:
  7.2 100.3 %copy-start.1 = (bf16[512,2048]{1,0:T(8,128)(2,1)S(1)}, bf16[512,2048]{1,0:T(8,128)(2,1)}, u32[]{:S(2)}) copy-start(bf16[512,2048]{1,0:T(8,128)(2,1)} %param.11) | copy-start | bytes 6291460
  7.2 191.2 %all-gather.6.cloned.1.call-start = ((), (), s32[]{:S(2)}) async-start(), calls=%async_computation.2 | async-start | bytes 7077888 | tf_op jit(solution)/shard_map/all_gather | solution.py:40
  7.9 281.8 %all-gather.4.cloned.1.call-start = ((), (), s32[]{:S(2)}) async-start(), calls=%async_computation.1 | async-start | bytes 7077888 | tf_op jit(solution)/shard_map/all_gather | solution.py:42
  8.7 487.6 %reduce-scatter.2.cloned.1.call-start = ((), (), s32[]{:S(2)}) async-start(), calls=%async_computation.4 | async-start | bytes 13369344 | tf_op jit(solution)/shard_map/reduce_scatter | solution.py:75
  8.7 45.4 %collective-permute-start = (bf16[256,1536]{1,0:T(8,128)(2,1)}, bf16[256,1536]{1,0:T(8,128)(2,1)S(1)}, u32[]{:S(2)}, u32[]{:S(2)}) collective-permute-start(bf16[256,1536]{1,0:T(8,128)(2,1)} %param.9), channel_id=1, source_target_pairs={{0,2},{2,4},{4,6},{6,8},{8,10},{10,12},{12,14},{14,0},{1,3},{3,5},... | collective-permute-start | bytes 2359304 | tf_op jit(solution)/shard_map/ppermute | solution.py:18
  11.8 44.8 %collective-permute-start.1 = (bf16[256,1536]{1,0:T(8,128)(2,1)}, bf16[256,1536]{1,0:T(8,128)(2,1)}, u32[]{:S(2)}, u32[]{:S(2)}) collective-permute-start(bf16[256,1536]{1,0:T(8,128)(2,1)} %param.9), channel_id=1, source_target_pairs={{0,14},{2,0},{4,2},{6,4},{8,6},{10,8},{12,10},{14,12},{1,15},{3,1}... | collective-permute-start | bytes 2359304 | tf_op jit(solution)/shard_map/ppermute | solution.py:23
  54.1 2.4 copy-start.5
  54.2 50.7 %collective-permute-start.2 = (bf16[256,1536]{1,0:T(8,128)(2,1)S(1)}, bf16[256,1536]{1,0:T(8,128)(2,1)}, u32[]{:S(2)}, u32[]{:S(2)}) collective-permute-start(bf16[256,1536]{1,0:T(8,128)(2,1)S(1)} %collective-permute-done), channel_id=1, source_target_pairs={{0,2},{2,4},{4,6},{6,8},{8,10},{10,12},{12,14},{14,0},{1,3},{3,5},... | collective-permute-start | bytes 2359304 | tf_op jit(solution)/shard_map/ppermute | solution.py:18
  56.5 57.9 %collective-permute-start.3 = (bf16[256,1536]{1,0:T(8,128)(2,1)}, bf16[256,1536]{1,0:T(8,128)(2,1)S(1)}, u32[]{:S(2)}, u32[]{:S(2)}) collective-permute-start(bf16[256,1536]{1,0:T(8,128)(2,1)} %collective-permute-done.1), channel_id=1, source_target_pairs={{0,14},{2,0},{4,2},{6,4},{8,6},{10,8},{12,10},{14,12},{1,15},{3,1}... | collective-permute-start | bytes 2359304 | tf_op jit(solution)/shard_map/ppermute | solution.py:23
  104.8 53.3 %collective-permute-start.4 = (bf16[256,1536]{1,0:T(8,128)(2,1)}, bf16[256,1536]{1,0:T(8,128)(2,1)}, u32[]{:S(2)}, u32[]{:S(2)}) collective-permute-start(bf16[256,1536]{1,0:T(8,128)(2,1)} %collective-permute-done.2), channel_id=1, source_target_pairs={{0,2},{2,4},{4,6},{6,8},{8,10},{10,12},{12,14},{14,0},{1,3},{3,5},... | collective-permute-start | bytes 2359304 | tf_op jit(solution)/shard_map/ppermute | solution.py:18
  113.0 1.1 copy-start.4
  113.0 1.4 copy-start.6
  114.5 54.5 %collective-permute-start.5 = (bf16[256,1536]{1,0:T(8,128)(2,1)S(1)}, bf16[256,1536]{1,0:T(8,128)(2,1)S(1)}, u32[]{:S(2)}, u32[]{:S(2)}) collective-permute-start(bf16[256,1536]{1,0:T(8,128)(2,1)S(1)} %collective-permute-done.3), channel_id=1, source_target_pairs={{0,14},{2,0},{4,2},{6,4},{8,6},{10,8},{12,10},{14,12},{1,15},{3,1}... | collective-permute-start | bytes 2359304 | tf_op jit(solution)/shard_map/ppermute | solution.py:23
  158.1 32.3 %collective-permute-start.6 = (bf16[256,1536]{1,0:T(8,128)(2,1)}, bf16[256,1536]{1,0:T(8,128)(2,1)S(1)}, u32[]{:S(2)}, u32[]{:S(2)}) collective-permute-start(bf16[256,1536]{1,0:T(8,128)(2,1)} %collective-permute-done.4), channel_id=1, source_target_pairs={{0,2},{2,4},{4,6},{6,8},{8,10},{10,12},{12,14},{14,0},{1,3},{3,5},... | collective-permute-start | bytes 2359304 | tf_op jit(solution)/shard_map/ppermute | solution.py:18
  161.8 31.4 %copy-start = (bf16[512,2048]{1,0:T(8,128)(2,1)S(1)}, bf16[512,2048]{1,0:T(8,128)(2,1)}, u32[]{:S(2)}) copy-start(bf16[512,2048]{1,0:T(8,128)(2,1)} %param.6) | copy-start | bytes 6291460
  161.8 31.4 %copy-start.7 = (f32[2048]{0:T(1024)S(1)}, f32[2048]{0:T(1024)}, u32[]{:S(2)}) copy-start(f32[2048]{0:T(1024)} %param.7) | copy-start | bytes 24580
  190.5 2.7 copy-start.2
  198.4 7.6 %copy-start.3 = (bf16[512,2,8,128]{0,3,2,1:T(8,128)(2,1)S(1)}, bf16[512,2,8,128]{0,3,2,1:T(8,128)(2,1)}, u32[]{:S(2)}) copy-start(bf16[512,2,8,128]{0,3,2,1:T(8,128)(2,1)} %copy.12) | copy-start | bytes 6291460
  198.4 7.6 %copy-start.8 = (f32[512,1536]{1,0:T(8,128)S(1)}, f32[512,1536]{1,0:T(8,128)}, u32[]{:S(2)}) copy-start(f32[512,1536]{1,0:T(8,128)} %fusion.16) | copy-start | bytes 9437188
  204.3 1.6 copy-start.10
  212.8 307.0 %all-reduce.2.cloned.1.call-start = ((), (), s32[]{:S(2)}) async-start(), calls=%async_computation.3 | async-start | bytes 4194304 | tf_op jit(solution)/shard_map/psum | solution.py:56
  289.7 8.6 %copy-start.9 = (f32[512,1536]{1,0:T(8,128)S(1)}, f32[512,1536]{1,0:T(8,128)}, u32[]{:S(2)}) copy-start(f32[512,1536]{1,0:T(8,128)} %fusion.16) | copy-start | bytes 9437188
  289.7 8.6 %copy-start.11 = (f32[512,1536]{1,0:T(8,128)S(1)}, f32[512,1536]{1,0:T(8,128)}, u32[]{:S(2)}) copy-start(f32[512,1536]{1,0:T(8,128)} %copy-done.10) | copy-start | bytes 9437188
  289.7 17.1 %slice-start = ((s8[6291456]{0:T(1024)(128)(4,1)}), s8[4194304]{0:T(1024)(128)(4,1)S(1)}, s32[]{:S(2)}) async-start(s8[6291456]{0:T(1024)(128)(4,1)} %bitcast.14), calls=%async_computation.6 | async-start | bytes 8388608
  298.3 8.5 %slice-start.1 = ((s8[6291456]{0:T(1024)(128)(4,1)}), s8[2097152]{0:T(1024)(128)(4,1)S(1)}, s32[]{:S(2)}) async-start(s8[6291456]{0:T(1024)(128)(4,1)} %bitcast.14), calls=%async_computation.7 | async-start | bytes 4194304
  313.5 257.6 %all-gather.8.cloned.1.call-start = ((), (), s32[]{:S(2)}) async-start(), calls=%async_computation.5 | async-start | bytes 2359296 | tf_op jit(solution)/shard_map/all_gather | solution.py:81
Sparse Core Ops, SparseCore 0:
  10.2 179.9 all-gather.5
  192.3 97.2 all-gather.3
  295.3 200.9 reduce-scatter.1
  499.0 20.7 all-reduce.1
  521.2 28.3 all-gather.7
